TPU v7x, 32 devices: a whole 2x2x4 slice. The times are simulated.
32 devices in a mesh: grp: 2 (over y), sp: 4 (over z), tp: 4 (over x, core).
Axes of the slice: x: 2, y: 2, z: 4, core: 2. Of those that a mesh axis runs over, the one named last changes fastest.
Arguments:
- tokens: bfloat16 [1024, 2048], P(('grp', 'sp')), parts along dimension 0, may hold values from -8 to 8
- norm_gain: float32 [2048], replicated, may hold values from 0.1 to 1.9
- w_query: bfloat16 [2048, 1024], P(None, 'tp'), may hold values from -0.125 to 0.125
- w_key: bfloat16 [2048, 1024], P(None, 'tp'), may hold values from -0.125 to 0.125
- w_value: bfloat16 [2048, 1024], P(None, 'tp'), may hold values from -0.125 to 0.125
- w_out: bfloat16 [1024, 2048], P('tp'), may hold values from -0.1875 to 0.1875
- key_rate: bfloat16 [16, 1024], P('tp', ('grp', 'sp')), parts along dimension 1, may hold values from -16 to 1
Outputs:
- layer_out: bfloat16 [1024, 2048], P(('grp', 'sp')), parts along dimension 0
There are 2 independent parts, one for each index of `grp`. A program takes and returns all parts, laid end to end along the dimension named above; an argument that names none is the same for every part. Nothing has to cross between parts.
All inputs are finite; a program needn't handle non-finite values.
Results may differ from a plain program's by a relative error of at most 0.0075.
Values may be sent and summed in bfloat16 or wider, within the bound.
No kernel may reach another device: no remote copies, remote signals or barrier semaphores. Data moves between devices by JAX's collectives and lax.ppermute only.
A program may use at most 64 MiB of HBM per device.

v0:
```python
import jax
import jax.numpy as jnp
from jax import lax
from jax.sharding import PartitionSpec as P

HD = 64
KEY_SPAN = 128


F32 = jnp.float32
BF16 = jnp.bfloat16
HIGHEST = lax.Precision.HIGHEST
EPS = 1e-06


def break_scores(query_heads, key_heads, rate_row_values, query_pos, key_pos):
    scores = jnp.einsum(
        "qhd,khd->hqk", query_heads, key_heads, preferred_element_type=F32
    ) * HD ** (-0.5)
    scores = scores + jnp.transpose(rate_row_values).astype(F32)[:, None, :]
    causal_mask = key_pos[None, :] < query_pos[:, None]
    log_remain = jnp.where(causal_mask[None], jax.nn.log_sigmoid(-scores), 0.0)
    return (scores, causal_mask, log_remain)


def shard_summary(query_heads, key_heads, value_heads, rate_row_values, query_pos, key_pos):
    scores, causal_mask, log_remain = break_scores(
        query_heads, key_heads, rate_row_values, query_pos, key_pos
    )
    heads_here, query_count, key_count = scores.shape
    span_count = key_count // KEY_SPAN
    blocks = log_remain.reshape(heads_here, query_count, span_count, KEY_SPAN)
    span_ids = jnp.arange(KEY_SPAN, dtype=jnp.int32)
    tri_strict = (span_ids[:, None] > span_ids[None, :]).astype(F32)
    inside_sum = jnp.einsum("hqnj,js->hqns", blocks, tri_strict, precision=HIGHEST)
    block_ids = jnp.arange(span_count, dtype=jnp.int32)
    block_later = (block_ids[:, None] > block_ids[None, :]).astype(F32)
    beyond = jnp.einsum("hqn,nm->hqm", jnp.sum(blocks, axis=-1), block_later, precision=HIGHEST)
    suffix = (inside_sum + beyond[..., None]).reshape(heads_here, query_count, key_count)
    weight = jnp.where(causal_mask[None], jnp.exp(jax.nn.log_sigmoid(scores) + suffix), 0.0).astype(
        BF16
    )
    partial_value = jnp.einsum("hqk,khd->qhd", weight, value_heads, preferred_element_type=F32)
    return (partial_value.reshape(query_count, heads_here * HD), jnp.sum(log_remain, axis=-1))


def on_device(tokens, norm_gain, w_query, w_key, w_value, w_out, key_rate):
    tokens_f = tokens.astype(F32)
    normed = (
        tokens_f
        * lax.rsqrt(jnp.mean(tokens_f * tokens_f, axis=-1, keepdims=True) + EPS)
        * norm_gain
    ).astype(BF16)
    queries = jnp.dot(normed, w_query, preferred_element_type=F32).astype(BF16)
    key_rows = jnp.dot(normed, w_key, preferred_element_type=F32).astype(BF16)
    value_rows = jnp.dot(normed, w_value, preferred_element_type=F32).astype(BF16)
    head_width = w_query.shape[1]
    heads_local = head_width // HD
    row_count = tokens.shape[0]
    rate_row_values = jnp.transpose(key_rate)
    query_heads = queries.reshape(row_count, heads_local, HD)
    own_shard = lax.axis_index("sp")
    shard_total = lax.axis_size("sp")
    local_pos = jnp.arange(row_count, dtype=jnp.int32)
    shard_ids = jnp.arange(shard_total, dtype=jnp.int32)
    later_mask = (shard_ids[:, None] > shard_ids[None, :]).astype(F32)
    query_groups = [(query_heads, own_shard * row_count)]

    def summarize(key_block, value_block, rate_block, first_key):
        key_pos = first_key + local_pos
        group_heads, group_start = query_groups[0]
        group_count = group_heads.shape[0]
        group_pos = group_start + jnp.arange(group_count, dtype=jnp.int32)
        empty_pair = (
            jnp.zeros((group_count, head_width), F32),
            jnp.zeros((heads_local, group_count), F32),
        )
        partial_value, remain = lax.cond(
            first_key < group_start + group_count - 1,
            lambda: shard_summary(
                group_heads, key_block, value_block, rate_block, group_pos, key_pos
            ),
            lambda: empty_pair,
        )
        partial_list = [partial_value]
        remain_list = [remain]
        return (jnp.concatenate(partial_list, axis=0), jnp.concatenate(remain_list, axis=1))

    initial = (
        jnp.zeros((shard_total, row_count, head_width), F32),
        jnp.zeros((shard_total, heads_local, row_count), F32),
    )
    piece_keys = lax.all_gather(key_rows, "sp", axis=0, tiled=True)
    piece_values = lax.all_gather(value_rows, "sp", axis=0, tiled=True)
    piece_rates = lax.all_gather(rate_row_values, "sp", axis=0, tiled=True)
    piece_count = piece_keys.shape[0] // row_count
    key_blocks = piece_keys.reshape(piece_count, row_count, heads_local, HD)
    value_blocks = piece_values.reshape(piece_count, row_count, heads_local, HD)
    rate_blocks = piece_rates.reshape(piece_count, row_count, heads_local)

    def absorb_one(inner_pair, item_tuple):
        item_index, key_block, value_block, rate_block = item_tuple
        first_key = item_index * row_count
        shard_index = first_key // row_count
        partial_value, remain = summarize(key_block, value_block, rate_block, first_key)
        partials = lax.dynamic_update_index_in_dim(inner_pair[0], partial_value, shard_index, 0)
        remains = lax.dynamic_update_index_in_dim(inner_pair[1], remain, shard_index, 0)
        return ((partials, remains), None)

    result, _ = lax.scan(
        absorb_one,
        initial,
        (jnp.arange(piece_count, dtype=jnp.int32), key_blocks, value_blocks, rate_blocks),
    )
    partials, remains = result
    beyond = jnp.einsum("nhq,nm->mhq", remains, later_mask, precision=HIGHEST)
    factor = jnp.transpose(jnp.exp(beyond), (0, 2, 1))[..., None]
    mixed_rows = jnp.sum(partials.reshape(shard_total, row_count, heads_local, HD) * factor, axis=0)
    mixed = mixed_rows.reshape(row_count, head_width).astype(BF16)
    token_heads = lax.all_to_all(mixed, "tp", split_axis=0, concat_axis=1, tiled=True)
    whole_out = lax.all_gather(w_out, "tp", axis=0, tiled=True)
    own_rows = jnp.dot(token_heads, whole_out, preferred_element_type=F32).astype(BF16)
    return lax.all_gather(own_rows, "tp", axis=0, tiled=True)


def solution(mesh):
    return jax.shard_map(
        on_device,
        mesh=mesh,
        in_specs=(
            P(("grp", "sp"), None),
            P(),
            P(None, "tp"),
            P(None, "tp"),
            P(None, "tp"),
            P("tp", None),
            P("tp", ("grp", "sp")),
        ),
        out_specs=P(("grp", "sp"), None),
        check_vma=False,
    )
```

profile of v0, /device:TPU:25, one launch (start us, length us, event | category | flops | bytes accessed | tf_op | source)
XLA Modules:
  0.0 93.3 jit_solution(17264272396755167459)
XLA Ops:
  6.5 0.7 all-gather.2.cloned.1.call-update
  7.3 1.2 %fusion.25 = f32[128]{0:T(128)S(1)} fusion(bf16[128,2048]{1,0:T(8,128)(2,1)} %param.11), kind=kLoop, calls=%fused_computation.40 | loop fusion | flops 786304 | bytes 524800 | tf_op jit(solution)/shard_map/reduce_sum | solution.py:51
  8.5 1.4 %convolution_convert_fusion.3 = bf16[128,256]{1,0:T(8,128)(2,1)S(1)} fusion(bf16[2048,256]{1,0:T(8,128)(2,1)S(1)} %copy-done, bf16[128,2048]{1,0:T(8,128)(2,1)} %param.11, f32[2048]{0:T(1024)} %param.12, f32[128]{0:T(128)S(1)} %add_rsqrt_fusion), kind=kOutput, calls=%fused_computation.37 | convolution fusion | flops 135299072 | bytes 1647104 | tf_op jit(solution)/shard_map/dot_general | solution.py:55
  9.9 11.0 %all_gather.15 = bf16[512,256]{1,0:T(8,128)(2,1)S(1)} all-gather(bf16[128,256]{1,0:T(8,128)(2,1)S(1)} %convolution_convert_fusion.3), channel_id=1, replica_groups=mesh['grp'=2,'sp'=4,'tp'=4] {'sp'}, dimensions={0}, use_global_device_ids=true | all-gather | bytes 327680 | tf_op jit(solution)/shard_map/all_gather | solution.py:93
  20.9 0.2 reshape.91
  21.2 0.3 copy.39
  21.5 1.6 %convolution_convert_fusion.1 = bf16[128,256]{1,0:T(8,128)(2,1)S(1)} fusion(bf16[2048,256]{1,0:T(8,128)(2,1)} %param.15, bf16[128,2048]{1,0:T(8,128)(2,1)S(1)} %copy-done.1, f32[2048]{0:T(1024)S(1)} %copy-done.3, f32[128]{0:T(128)S(1)} %add_rsqrt_fusion), kind=kOutput, calls=%fused_computation.35 | convolution fusion | flops 135299072 | bytes 1647104 | tf_op jit(solution)/shard_map/dot_general | solution.py:56
  23.1 12.0 %all_gather.17 = bf16[512,256]{1,0:T(8,128)(2,1)S(1)} all-gather(bf16[128,256]{1,0:T(8,128)(2,1)S(1)} %convolution_convert_fusion.1), channel_id=1, replica_groups=mesh['grp'=2,'sp'=4,'tp'=4] {'sp'}, dimensions={0}, use_global_device_ids=true | all-gather | bytes 327680 | tf_op jit(solution)/shard_map/all_gather | solution.py:94
  35.1 0.2 reshape.92
  35.3 0.3 copy.40
  35.6 1.6 %convolution_convert_fusion.2 = bf16[128,256]{1,0:T(8,128)(2,1)S(1)} fusion(bf16[2048,256]{1,0:T(8,128)(2,1)} %param.13, bf16[128,2048]{1,0:T(8,128)(2,1)S(1)} %copy-done.1, f32[2048]{0:T(1024)S(1)} %copy-done.3, f32[128]{0:T(128)S(1)} %add_rsqrt_fusion), kind=kOutput, calls=%fused_computation.36 | convolution fusion | flops 135299072 | bytes 1647104 | tf_op jit(solution)/shard_map/dot_general | solution.py:54
  37.2 0.1 copy.37
  37.3 5.6 %all_gather.16 = bf16[512,4]{0,1:T(4,128)(2,1)S(1)} all-gather(bf16[128,4]{0,1:T(4,128)(2,1)S(1)} %bitcast.58), channel_id=1, replica_groups=mesh['grp'=2,'sp'=4,'tp'=4] {'sp'}, dimensions={0}, use_global_device_ids=true | all-gather | bytes 5120 | tf_op jit(solution)/shard_map/all_gather | solution.py:95
  43.0 18.4 %while.16 = (s32[]{:T(128)}, f32[4,128,256]{1,2,0:T(8,128)S(1)}, f32[4,4,128]{2,0,1:T(4,128)S(1)}, s32[4]{0:T(128)S(1)}, s32[]{:T(128)}, /*index=5*/s32[]{:T(128...) while((s32[]{:T(128)}, f32[4,128,256]{1,2,0:T(8,128)S(1)}, ...), condition=%wide.region_5.6_spmd.clone, body=%wide.region_1.5_spmd.clone.sunk | while | flops 119505664 | bytes 1446895 | solution.py:110
  43.0 0.6 dynamic_slice.50
  44.3 2.6 %conditional.3 = (f32[1,128,256]{1,2,0:T(8,128)S(1)}, f32[1,4,128]{2,1,0:T(4,128)}) conditional(s32[]{:T(128)} %convert_element_type.82, () %tuple.61, (s32[]{:T(128)}, s32[128]{0:T(128)S(1)}, s32[]{:T(128)}, s32[128]{0:T(128)S(1)}, bf16[4,128,4,64]{1,3,2,0:T(8,128)(2,1)S(1)}, /*index=5*/s32[]{:T(128)}, bf16[128,4,64]{0,2,1:T(8,128)(2,1)S(1)}, ...), branch_computations={%region_2.2_spmd, %region_3.4_spmd} | conditional | flops 119505664 | bytes 1179684 | solution.py:78
  44.4 1.0 %fusion.11 = (f32[4,128]{1,0:T(4,128)}, f32[4,128,128]{1,2,0:T(8,128)S(1)}) fusion(pred[128,128]{0,1:T(8,128)(4,1)S(1)} %broadcast_compare_fusion, f32[4,128]{1,0:T(4,128)S(1)} %convert_bitcast_fusion, bf16[128,4,64]{0,2,1:T(8,128)(2,1)S(1)} %get-tuple-element.246, bf16[4,128,4,64]{1,3,2,0:T(8,128)(2,1)S(1)} %get-tuple-element.244, s32[]{:T(128)} %get-tuple-element.245), kind=kOutput, calls=%fused_computation.14 | convolution fusion | flops 9108992 | bytes 413700 | tf_op jit(solution)/shard_map/while/body/eval_jaxpr/cond/branch_1_fun/qhd,khd->hqk/dot_general | solution.py:17
  45.4 0.7 broadcast_multiply_fusion
  46.1 0.6 fusion.7
  46.7 0.2 fusion.14
  46.9 0.7 dynamic_update_slice.22
  47.6 0.6 dynamic_slice.50
  48.9 2.6 %conditional.3 = (f32[1,128,256]{1,2,0:T(8,128)S(1)}, f32[1,4,128]{2,1,0:T(4,128)}) conditional(s32[]{:T(128)} %convert_element_type.82, () %tuple.61, (s32[]{:T(128)}, s32[128]{0:T(128)S(1)}, s32[]{:T(128)}, s32[128]{0:T(128)S(1)}, bf16[4,128,4,64]{1,3,2,0:T(8,128)(2,1)S(1)}, /*index=5*/s32[]{:T(128)}, bf16[128,4,64]{0,2,1:T(8,128)(2,1)S(1)}, ...), branch_computations={%region_2.2_spmd, %region_3.4_spmd} | conditional | flops 119505664 | bytes 1179684 | solution.py:78
  49.0 1.0 %fusion.11 = (f32[4,128]{1,0:T(4,128)}, f32[4,128,128]{1,2,0:T(8,128)S(1)}) fusion(pred[128,128]{0,1:T(8,128)(4,1)S(1)} %broadcast_compare_fusion, f32[4,128]{1,0:T(4,128)S(1)} %convert_bitcast_fusion, bf16[128,4,64]{0,2,1:T(8,128)(2,1)S(1)} %get-tuple-element.246, bf16[4,128,4,64]{1,3,2,0:T(8,128)(2,1)S(1)} %get-tuple-element.244, s32[]{:T(128)} %get-tuple-element.245), kind=kOutput, calls=%fused_computation.14 | convolution fusion | flops 9108992 | bytes 413700 | tf_op jit(solution)/shard_map/while/body/eval_jaxpr/cond/branch_1_fun/qhd,khd->hqk/dot_general | solution.py:17
  50.0 0.7 broadcast_multiply_fusion
  50.7 0.6 fusion.7
  51.3 0.2 fusion.14
  51.5 0.7 dynamic_update_slice.22
  52.2 0.6 dynamic_slice.50
  53.5 2.6 %conditional.3 = (f32[1,128,256]{1,2,0:T(8,128)S(1)}, f32[1,4,128]{2,1,0:T(4,128)}) conditional(s32[]{:T(128)} %convert_element_type.82, () %tuple.61, (s32[]{:T(128)}, s32[128]{0:T(128)S(1)}, s32[]{:T(128)}, s32[128]{0:T(128)S(1)}, bf16[4,128,4,64]{1,3,2,0:T(8,128)(2,1)S(1)}, /*index=5*/s32[]{:T(128)}, bf16[128,4,64]{0,2,1:T(8,128)(2,1)S(1)}, ...), branch_computations={%region_2.2_spmd, %region_3.4_spmd} | conditional | flops 119505664 | bytes 1179684 | solution.py:78
  53.6 1.0 %fusion.11 = (f32[4,128]{1,0:T(4,128)}, f32[4,128,128]{1,2,0:T(8,128)S(1)}) fusion(pred[128,128]{0,1:T(8,128)(4,1)S(1)} %broadcast_compare_fusion, f32[4,128]{1,0:T(4,128)S(1)} %convert_bitcast_fusion, bf16[128,4,64]{0,2,1:T(8,128)(2,1)S(1)} %get-tuple-element.246, bf16[4,128,4,64]{1,3,2,0:T(8,128)(2,1)S(1)} %get-tuple-element.244, s32[]{:T(128)} %get-tuple-element.245), kind=kOutput, calls=%fused_computation.14 | convolution fusion | flops 9108992 | bytes 413700 | tf_op jit(solution)/shard_map/while/body/eval_jaxpr/cond/branch_1_fun/qhd,khd->hqk/dot_general | solution.py:17
  54.6 0.7 broadcast_multiply_fusion
  55.3 0.6 fusion.7
  55.9 0.2 fusion.14
  56.1 0.7 dynamic_update_slice.22
  56.8 0.6 dynamic_slice.50
  58.1 2.6 %conditional.3 = (f32[1,128,256]{1,2,0:T(8,128)S(1)}, f32[1,4,128]{2,1,0:T(4,128)}) conditional(s32[]{:T(128)} %convert_element_type.82, () %tuple.61, (s32[]{:T(128)}, s32[128]{0:T(128)S(1)}, s32[]{:T(128)}, s32[128]{0:T(128)S(1)}, bf16[4,128,4,64]{1,3,2,0:T(8,128)(2,1)S(1)}, /*index=5*/s32[]{:T(128)}, bf16[128,4,64]{0,2,1:T(8,128)(2,1)S(1)}, ...), branch_computations={%region_2.2_spmd, %region_3.4_spmd} | conditional | flops 119505664 | bytes 1179684 | solution.py:78
  58.2 1.0 %fusion.11 = (f32[4,128]{1,0:T(4,128)}, f32[4,128,128]{1,2,0:T(8,128)S(1)}) fusion(pred[128,128]{0,1:T(8,128)(4,1)S(1)} %broadcast_compare_fusion, f32[4,128]{1,0:T(4,128)S(1)} %convert_bitcast_fusion, bf16[128,4,64]{0,2,1:T(8,128)(2,1)S(1)} %get-tuple-element.246, bf16[4,128,4,64]{1,3,2,0:T(8,128)(2,1)S(1)} %get-tuple-element.244, s32[]{:T(128)} %get-tuple-element.245), kind=kOutput, calls=%fused_computation.14 | convolution fusion | flops 9108992 | bytes 413700 | tf_op jit(solution)/shard_map/while/body/eval_jaxpr/cond/branch_1_fun/qhd,khd->hqk/dot_general | solution.py:17
  59.2 0.7 broadcast_multiply_fusion
  59.9 0.6 fusion.7
  60.5 0.2 fusion.14
  60.7 0.7 dynamic_update_slice.22
  61.4 0.1 fusion.24
  61.6 0.1 copy.43
  61.7 13.7 %all_to_all.16 = bf16[4,32,256]{2,1,0:T(8,128)(2,1)S(1)} all-to-all(bf16[4,32,256]{2,1,0:T(8,128)(2,1)S(1)} %bitcast.54), channel_id=1, replica_groups=mesh['grp'=2,'sp'=4,'tp'=4] {'tp'}, dimensions={0} | all-to-all | bytes 131072 | tf_op jit(solution)/shard_map/all_to_all | solution.py:120
  75.4 3.0 %convolution_convert_fusion = bf16[32,2048]{1,0:T(8,128)(2,1)S(1)} fusion(bf16[32,1024]{1,0:T(8,128)(2,1)S(1)} %bitcast.53, bf16[1024,2048]{1,0:T(8,128)(2,1)} %all-gather.2.cloned.1.call-done), kind=kOutput, calls=%fused_computation.32 | convolution fusion | flops 134283264 | bytes 4390912 | tf_op jit(solution)/shard_map/dot_general | solution.py:122
  78.4 7.3 %all_gather.19 = bf16[128,2048]{1,0:T(8,128)(2,1)S(1)} all-gather(bf16[32,2048]{1,0:T(8,128)(2,1)S(1)} %convolution_convert_fusion), channel_id=1, replica_groups=mesh['grp'=2,'sp'=4,'tp'=4] {'tp'}, dimensions={0}, use_global_device_ids=true | all-gather | bytes 655360 | tf_op jit(solution)/shard_map/all_gather | solution.py:123
  85.7 0.8 copy.73
  (37 shorter events, 0.6 us)
Async XLA Ops:
  6.5 2.0 %copy-start = (bf16[2048,256]{1,0:T(8,128)(2,1)S(1)}, bf16[2048,256]{1,0:T(8,128)(2,1)}, u32[]{:S(2)}) copy-start(bf16[2048,256]{1,0:T(8,128)(2,1)} %param.14) | copy-start | bytes 3145732
  6.5 14.9 %copy-start.1 = (bf16[128,2048]{1,0:T(8,128)(2,1)S(1)}, bf16[128,2048]{1,0:T(8,128)(2,1)}, u32[]{:S(2)}) copy-start(bf16[128,2048]{1,0:T(8,128)(2,1)} %param.11) | copy-start | bytes 1572868
  6.5 14.9 %copy-start.3 = (f32[2048]{0:T(1024)S(1)}, f32[2048]{0:T(1024)}, u32[]{:S(2)}) copy-start(f32[2048]{0:T(1024)} %param.12) | copy-start | bytes 24580
  6.5 68.8 %all-gather.2.cloned.1.call-start = ((), (), s32[]{:S(2)}) async-start(), calls=%async_computation.1 | async-start | bytes 5242880 | tf_op jit(solution)/shard_map/all_gather | solution.py:121
  9.9 27.4 %copy-start.2 = (bf16[4,128]{1,0:T(4,128)(2,1)S(1)}, bf16[4,128]{1,0:T(4,128)(2,1)}, u32[]{:S(2)}) copy-start(bf16[4,128]{1,0:T(4,128)(2,1)} %param.17) | copy-start | bytes 3076
Sparse Core Ops, SparseCore 0:
  8.9 35.8 all-gather.1
where the time goes:
time: 93.8 us; the launch traced here: 93.3 us
  blocking collectives  49.5 us (53%)
  matrix products  14.6 us (16%)
  between operations  13.5 us (14%)
  local copies, waits for them, and re-layouts  7.46 us (8%)
  other arithmetic  4.42 us (5%)
  loops' own time  3.02 us (3%)
    all_to_all x1, blocking collectives, on_device(): lax.all_to_all(mixed, 'tp', split_axis=0, concat_axis=1, tiled=True)  13.7 us
    all_gather x1, blocking collectives, on_device(): piece_values = lax.all_gather(value_rows, 'sp', axis=0, tiled=True)  12 us
    all_gather x1, blocking collectives, on_device(): piece_keys = lax.all_gather(key_rows, 'sp', axis=0, tiled=True)  11 us
    all_gather x1, blocking collectives, on_device(): return lax.all_gather(own_rows, 'tp', axis=0, tiled=True)  7.28 us
    all_gather x1, blocking collectives, on_device(): piece_rates = lax.all_gather(rate_row_values, 'sp', axis=0, tiled=True)  5.6 us
    dot_general x4, matrix products, break_scores(): jnp.einsum('qhd,khd->hqk', query_heads, key_heads, preferred_element_type...  3.93 us
    dot_general x1, matrix products, on_device(): jnp.dot(token_heads, whole_out, preferred_element_type=F32).astype(BF16)  3.01 us
    dynamic_update_slice x4, local copies, waits for them, and re-layouts, absorb_one(): lax.dynamic_update_index_in_dim(inner_pair[1], remain, shard_index, 0)  2.88 us
  transfers between devices with their start and end apart: 1, of which 0 were waited for; matrix products, arithmetic and copies ran while one was open for 24% of the time, Pallas kernels for 0%

commit v1 on v0

v1 whole, which is shorter than its diff:
```python
import functools

import jax
import jax.numpy as jnp
from jax import lax
from jax.experimental import pallas as pl
from jax.experimental.pallas import tpu as pltpu
from jax.sharding import PartitionSpec as P

HD = 64
EPS = 1e-06
F32 = jnp.float32
BF16 = jnp.bfloat16
VMEM_SPEC = pl.BlockSpec(memory_space=pltpu.VMEM)
HBM_SPEC = pl.BlockSpec(memory_space=pltpu.HBM)


def project_kernel(chunks, tok_hbm, gain_ref, rate_ref, wk_hbm, wv_hbm, wq_hbm, kv_ref, q_ref, tok, w, normed, tok_sem, w_sem):
    rows, model = tok.shape
    width = q_ref.shape[1]
    depth = model // chunks
    tok_copy = pltpu.make_async_copy(tok_hbm, tok, tok_sem)
    tok_copy.start()
    copies = []
    for i, ref in enumerate((wk_hbm, wv_hbm, wq_hbm)):
        for c in range(chunks):
            copy = pltpu.make_async_copy(
                ref.at[pl.ds(c * depth, depth)], w.at[i, pl.ds(c * depth, depth)], w_sem.at[i, c]
            )
            copy.start()
            copies.append(copy)
    tok_copy.wait()
    values = tok[...].astype(F32)
    scale = lax.rsqrt(jnp.mean(values * values, axis=-1, keepdims=True) + EPS)
    normed[...] = (values * scale * gain_ref[...]).astype(BF16)
    for i in range(3):
        total = jnp.zeros((rows, width), F32)
        for c in range(chunks):
            copies[i * chunks + c].wait()
            total += jnp.dot(
                normed[:, pl.ds(c * depth, depth)],
                w[i, pl.ds(c * depth, depth)],
                preferred_element_type=F32,
            )
        out = total.astype(BF16)
        if i < 2:
            kv_ref[pl.ds(0, rows), pl.ds(i * width, width)] = out
        else:
            q_ref[...] = out * jnp.asarray(HD**-0.5, BF16)
    pad = jnp.zeros((kv_ref.shape[0] - rows, 2 * width), BF16)
    kv_ref[pl.ds(rows, kv_ref.shape[0] - rows), :] = pad
    heads = rate_ref.shape[0]
    kv_ref[pl.ds(rows, heads), pl.ds(0, rows)] = rate_ref[...]


def project(tokens, gain, rate, w_key, w_value, w_query):
    rows, model = tokens.shape
    width = w_query.shape[1]
    chunks = 4
    rate_rows = -(-rate.shape[0] // 8) * 8
    return pl.pallas_call(
        functools.partial(project_kernel, chunks),
        out_shape=(
            jax.ShapeDtypeStruct((rows + rate_rows, 2 * width), BF16),
            jax.ShapeDtypeStruct((rows, width), BF16),
        ),
        in_specs=[HBM_SPEC, VMEM_SPEC, VMEM_SPEC, HBM_SPEC, HBM_SPEC, HBM_SPEC],
        out_specs=(VMEM_SPEC, VMEM_SPEC),
        scratch_shapes=[
            pltpu.VMEM((rows, model), BF16),
            pltpu.VMEM((3, model, width), BF16),
            pltpu.VMEM((rows, model), BF16),
            pltpu.SemaphoreType.DMA,
            pltpu.SemaphoreType.DMA((3, chunks)),
        ],
        cost_estimate=pl.CostEstimate(flops=6 * rows * model * width, bytes_accessed=6 * model * width, transcendentals=0),
        compiler_params=pltpu.CompilerParams(vmem_limit_bytes=8 << 20),
        name="project",
    )(tokens, gain.reshape(1, model), rate, w_key, w_value, w_query)


def attend_kernel(diagonal, q_ref, kv_ref, *refs):
    if diagonal:
        acc_out, rest_out = refs
    else:
        acc_in, rest_in, acc_out, rest_out = refs
    rows, width = q_ref.shape
    heads = width // HD
    q = q_ref[...]
    lane = lax.broadcasted_iota(jnp.int32, (rows, width), 1) // HD
    stacked = jnp.concatenate([jnp.where(lane == h, q, jnp.zeros_like(q)) for h in range(heads)], axis=0)
    keys = kv_ref[pl.ds(0, rows), pl.ds(0, width)]
    values = kv_ref[pl.ds(0, rows), pl.ds(width, width)]
    scores = lax.dot_general(stacked, keys, (((1,), (1,)), ((), ())), preferred_element_type=F32)
    rate = kv_ref[pl.ds(rows, heads), pl.ds(0, rows)].astype(F32)
    scores = jnp.concatenate(
        [scores[h * rows : (h + 1) * rows] + rate[h : h + 1] for h in range(heads)], axis=0
    )
    softened = jnp.log(1.0 + jnp.exp(-jnp.abs(scores)))
    log_keep = jnp.minimum(scores, 0.0) - softened
    log_remain = -jnp.maximum(scores, 0.0) - softened
    if diagonal:
        q_pos = lax.broadcasted_iota(jnp.int32, (heads * rows, rows), 0) % rows
        k_pos = lax.broadcasted_iota(jnp.int32, (heads * rows, rows), 1)
        mask = k_pos < q_pos
        log_remain = jnp.where(mask, log_remain, 0.0)
    high = log_remain.astype(BF16)
    low = (log_remain - high.astype(F32)).astype(BF16)
    from_pos = lax.broadcasted_iota(jnp.int32, (2 * rows, 2 * rows), 0) % rows
    to_pos = lax.broadcasted_iota(jnp.int32, (2 * rows, 2 * rows), 1)
    later = ((from_pos > to_pos) | (to_pos >= rows)).astype(F32).astype(BF16)
    sums = jnp.dot(jnp.concatenate([high, low], axis=1), later, preferred_element_type=F32)
    exponent = log_keep + sums[:, :rows]
    rest = sums[:, rows:]
    if not diagonal:
        exponent = exponent + rest_in[...]
        rest = rest + rest_in[...]
    weight = jnp.exp(exponent)
    if diagonal:
        weight = jnp.where(mask, weight, 0.0)
    weight = weight.astype(BF16)
    spread = jnp.dot(weight, values, preferred_element_type=F32)
    acc = jnp.zeros((rows, width), F32) if diagonal else acc_in[...]
    for h in range(heads):
        acc = acc + jnp.where(lane == h, spread[h * rows : (h + 1) * rows], 0.0)
    acc_out[...] = acc.astype(acc_out.dtype)
    rest_out[...] = rest


def attend(q, kv, state, last):
    rows, width = q.shape
    heads = width // HD
    diagonal = state is None
    operands = (q, kv) if diagonal else (q, kv, *state)
    return pl.pallas_call(
        functools.partial(attend_kernel, diagonal),
        out_shape=(
            jax.ShapeDtypeStruct((rows, width), BF16 if last else F32),
            jax.ShapeDtypeStruct((heads * rows, rows), F32),
        ),
        in_specs=[VMEM_SPEC] * len(operands),
        out_specs=(VMEM_SPEC, VMEM_SPEC),
        cost_estimate=pl.CostEstimate(flops=1000000000, bytes_accessed=1000000, transcendentals=0),
        compiler_params=pltpu.CompilerParams(vmem_limit_bytes=8 << 20),
        name="attend",
    )(*operands)


def output_kernel(count, *refs):
    out_ref = refs[-1]
    total = jnp.zeros(out_ref.shape, F32)
    for i in range(count):
        total += jnp.dot(refs[i][...], refs[count + i][...], preferred_element_type=F32)
    out_ref[...] = total.astype(BF16)


def output(mixed, weights):
    rows = mixed[0].shape[0]
    model = weights[0].shape[1]
    count = len(mixed)
    block = 512
    return pl.pallas_call(
        functools.partial(output_kernel, count),
        grid=(model // block,),
        out_shape=jax.ShapeDtypeStruct((rows, model), BF16),
        in_specs=[pl.BlockSpec(m.shape, lambda j: (0, 0)) for m in mixed]
        + [pl.BlockSpec((w.shape[0], block), lambda j: (0, j)) for w in weights],
        out_specs=pl.BlockSpec((rows, block), lambda j: (0, j)),
        cost_estimate=pl.CostEstimate(flops=2000000000, bytes_accessed=4000000, transcendentals=0),
        compiler_params=pltpu.CompilerParams(vmem_limit_bytes=12 << 20),
        name="output",
    )(*mixed, *weights)


def on_device(tokens, norm_gain, w_query, w_key, w_value, w_out, key_rate):
    shards = lax.axis_size("sp")
    group = lax.axis_size("tp")

    def swap(x, bit):
        return lax.ppermute(x, "tp", [(i, i ^ bit) for i in range(group)])

    bits = []
    while 2 << len(bits) <= group:
        bits.append(1 << len(bits))
    bits = bits[::-1]
    weights = [w_out]
    for bit in bits[:-1]:
        weights = weights + [swap(w, bit) for w in weights]
    near = swap(w_out, bits[-1])

    kv, q = project(tokens, norm_gain, key_rate, w_key, w_value, w_query)
    arrived = [
        lax.ppermute(kv, "sp", [(i, i + d) for i in range(shards - d)]) for d in range(1, shards)
    ]
    state = attend(q, kv, None, shards == 1)
    for d, block in enumerate(arrived):
        state = attend(q, block, state, d == shards - 2)
    mixed = [state[0]]
    weights += [near] + [swap(lax.optimization_barrier((w, state[0]))[0], bits[-1]) for w in weights[1:]]
    for bit in bits:
        joined = mixed[0] if len(mixed) == 1 else jnp.concatenate(mixed, axis=1)
        other = swap(joined, bit)
        width = mixed[0].shape[1]
        mixed = mixed + [other[:, i * width : (i + 1) * width] for i in range(len(mixed))]
    return output(mixed, weights)


def solution(mesh):
    return jax.shard_map(
        on_device,
        mesh=mesh,
        in_specs=(
            P(("grp", "sp"), None),
            P(),
            P(None, "tp"),
            P(None, "tp"),
            P(None, "tp"),
            P("tp", None),
            P("tp", ("grp", "sp")),
        ),
        out_specs=P(("grp", "sp"), None),
        check_vma=False,
    )
```

time: 93.8 us -> 35.9 us (0.38)
  blocking collectives: 49.5 us -> 0 us
  matrix products: 14.6 us -> 0 us
  between operations: 13.5 us -> 0.11 us
  waiting for transfers between devices: 0.71 us -> 13.5 us
  starting transfers between devices: 0.01 us -> 8.85 us
  Pallas kernels: 0 us -> 7.63 us
  other arithmetic: 4.42 us -> 0.01 us
  loops' own time: 3.02 us -> 0 us
  local copies, waits for them, and re-layouts: 7.46 us -> 5.43 us
    all_gather x4 -> x0, blocking collectives: 35.9 us -> none  [the longest x1 12 us: on_device(): piece_values = lax.all_gather(value_rows, 'sp', axis=0, tiled=True)]
    dot_general x17 -> x0, matrix products: 14.6 us -> none  [the longest x4 3.93 us: break_scores(): jnp.einsum('qhd,khd->hqk', query_heads, key_heads, preferred_element_type...]
    all_to_all x1 -> x0, blocking collectives: 13.7 us -> none  [on_device(): lax.all_to_all(mixed, 'tp', split_axis=0, concat_axis=1, tiled=True)]
    ppermute x0 -> x8, waiting for transfers between devices: none -> 13.5 us  [the longest x3 9.57 us: on_device(): lax.ppermute(kv, 'sp', [(i, i + d) for i in range(shards - d)])]
    ppermute x0 -> x8, starting transfers between devices: none -> 8.85 us  [the longest x5 4.97 us: swap(): return lax.ppermute(x, 'tp', [(i, i ^ bit) for i in range(group)])]
    pallas_call x0 -> x6, Pallas kernels: none -> 7.63 us  [the longest x4 2.88 us: attend(): pl.pallas_call(functools.partial(attend_kernel, diagonal), out_shape=(jax...]
    unnamed x11 -> x14, local copies, waits for them, and re-layouts: 1.36 us -> 5.42 us
    another operation x5 -> x0, loops' own time: 3.02 us -> none  [the longest x1 2.83 us: on_device(): lax.scan(absorb_one, initial, (jnp.arange(piece_count, dtype=jnp.int32),...]
  transfers between devices with their start and end apart: 1 -> 8, of which waited for: 0 -> 4; matrix products, arithmetic and copies ran while one was open for 24% -> 0% of each run, Pallas kernels for 0% -> 14%
where the time goes in v1:
time: 35.9 us; the launch traced here: 35.6 us
  waiting for transfers between devices  13.5 us (38%)
  starting transfers between devices  8.85 us (25%)
  Pallas kernels  7.63 us (21%)
  local copies, waits for them, and re-layouts  5.43 us (15%)
    ppermute x3, waiting for transfers between devices, on_device(): lax.ppermute(kv, 'sp', [(i, i + d) for i in range(shards - d)])  9.57 us
    unnamed x14, local copies, waits for them, and re-layouts  5.42 us
    ppermute x5, starting transfers between devices, swap(): return lax.ppermute(x, 'tp', [(i, i ^ bit) for i in range(group)])  4.97 us
    ppermute x5, waiting for transfers between devices, swap(): return lax.ppermute(x, 'tp', [(i, i ^ bit) for i in range(group)])  3.97 us
    ppermute x3, starting transfers between devices, on_device(): lax.ppermute(kv, 'sp', [(i, i + d) for i in range(shards - d)])  3.88 us
    pallas_call x4, Pallas kernels, attend(): pl.pallas_call(functools.partial(attend_kernel, diagonal), out_shape=(jax...  2.88 us
    pallas_call x1, Pallas kernels, output(): pl.pallas_call(functools.partial(output_kernel, count), grid=(model // bl...  2.53 us
    pallas_call x1, Pallas kernels, project(): pl.pallas_call(functools.partial(project_kernel, chunks), out_shape=(jax....  2.22 us
  transfers between devices with their start and end apart: 8, of which 4 were waited for; matrix products, arithmetic and copies ran while one was open for 0% of the time, Pallas kernels for 14%

profile of v1, /device:TPU:25, one launch (start us, length us, event | category | flops | bytes accessed | tf_op | source)
XLA Modules:
  0.0 35.6 jit_solution(8735584106750756956)
XLA Ops:
  0.0 0.0 copy-start.5
  0.0 1.2 %collective-permute-start.5 = (bf16[256,2048]{1,0:T(8,128)(2,1)}, bf16[256,2048]{1,0:T(8,128)(2,1)S(1)}, u32[]{:S(2)}, u32[]{:S(2)}) collective-permute-start(bf16[256,2048]{1,0:T(8,128)(2,1)} %refs_4_.1), channel_id=1, source_target_pairs={{0,2},{1,3},{2,0},{3,1},{4,6},{5,7},{6,4},{7,5},{8,10},{9,11},{10,... | collective-permute-start | bytes 3145736 | tf_op jit(solution)/shard_map/ppermute | solution.py:180
  1.2 0.0 copy-done.5
  1.2 0.0 copy-start
  1.2 1.2 %copy-done = bf16[2048,256]{1,0:T(8,128)(2,1)S(1)} copy-done((bf16[2048,256]{1,0:T(8,128)(2,1)S(1)}, bf16[2048,256]{1,0:T(8,128)(2,1)}, u32[]{:S(2)}) %copy-start) | copy-done | bytes 1048600
  2.4 0.0 copy-start.1
  2.4 1.2 %copy-done.1 = bf16[2048,256]{1,0:T(8,128)(2,1)S(1)} copy-done((bf16[2048,256]{1,0:T(8,128)(2,1)S(1)}, bf16[2048,256]{1,0:T(8,128)(2,1)}, u32[]{:S(2)}) %copy-start.1) | copy-done | bytes 1048600
  3.7 0.0 copy-start.2
  3.7 1.2 %copy-done.2 = bf16[2048,256]{1,0:T(8,128)(2,1)S(1)} copy-done((bf16[2048,256]{1,0:T(8,128)(2,1)S(1)}, bf16[2048,256]{1,0:T(8,128)(2,1)}, u32[]{:S(2)}) %copy-start.2) | copy-done | bytes 1048600
  4.9 0.0 copy-start.3
  4.9 1.0 %copy-done.3 = bf16[128,2048]{1,0:T(8,128)(2,1)S(1)} copy-done((bf16[128,2048]{1,0:T(8,128)(2,1)S(1)}, bf16[128,2048]{1,0:T(8,128)(2,1)}, u32[]{:S(2)}) %copy-start.3) | copy-done | bytes 524312
  5.9 0.0 copy-start.4
  5.9 0.7 %copy-done.4 = f32[2048]{0:T(1024)S(1)} copy-done((f32[2048]{0:T(1024)S(1)}, f32[2048]{0:T(1024)}, u32[]{:S(2)}) %copy-start.4) | copy-done | bytes 8216
  6.6 0.0 copy-start.6
  6.6 2.2 %project.1 = (bf16[136,512]{1,0:T(8,128)(2,1)S(1)}, bf16[128,256]{1,0:T(8,128)(2,1)S(1)}) custom-call(bf16[128,2048]{1,0:T(8,128)(2,1)S(1)} %copy-done.3, f32[1,2048]{1,0:T(1,128)S(1)} %bitcast.1, bf16[4,128]{1,0:T(4,128)(2,1)S(1)} %copy-done.5, bf16[2048,256]{1,0:T(8,128)(2,1)S(1)} %copy-done, bf16[2048,256]{1,0:T(8,128)(2,1)S(1)} %copy-done.1, ...), custom_call_target="tpu_custom_call" | custom-call | flops 402653184 | bytes 3145728 | tf_op jit(solution)/shard_map/project/pallas_call | solution.py:61
  8.9 1.3 %collective-permute-start.2 = (bf16[136,512]{1,0:T(8,128)(2,1)S(1)}, bf16[136,512]{1,0:T(8,128)(2,1)S(1)}, u32[]{:S(2)}, u32[]{:S(2)}) collective-permute-start(bf16[136,512]{1,0:T(8,128)(2,1)S(1)} %get-tuple-element.16.kv_ref), channel_id=1, source_target_pairs={{0,4},{4,8},{8,12},{1,5},{5,9},{9,13},{2,6},{6,10},{10,14},{3,7},{... | collective-permute-start | bytes 417800 | tf_op jit(solution)/shard_map/ppermute | solution.py:193
  10.2 1.3 %collective-permute-start.1 = (bf16[136,512]{1,0:T(8,128)(2,1)S(1)}, bf16[136,512]{1,0:T(8,128)(2,1)S(1)}, u32[]{:S(2)}, u32[]{:S(2)}) collective-permute-start(bf16[136,512]{1,0:T(8,128)(2,1)S(1)} %get-tuple-element.16.kv_ref), channel_id=1, source_target_pairs={{0,8},{4,12},{1,9},{5,13},{2,10},{6,14},{3,11},{7,15},{16,24},{20,... | collective-permute-start | bytes 417800 | tf_op jit(solution)/shard_map/ppermute | solution.py:193
  11.5 1.3 %collective-permute-start = (bf16[136,512]{1,0:T(8,128)(2,1)S(1)}, bf16[136,512]{1,0:T(8,128)(2,1)S(1)}, u32[]{:S(2)}, u32[]{:S(2)}) collective-permute-start(bf16[136,512]{1,0:T(8,128)(2,1)S(1)} %get-tuple-element.16.kv_ref), channel_id=1, source_target_pairs={{0,12},{1,13},{2,14},{3,15},{16,28},{17,29},{18,30},{19,31}} | collective-permute-start | bytes 417800 | tf_op jit(solution)/shard_map/ppermute | solution.py:193
  12.8 0.0 copy-done.6
  12.8 1.0 %collective-permute-start.6 = (bf16[256,2048]{1,0:T(8,128)(2,1)S(1)}, bf16[256,2048]{1,0:T(8,128)(2,1)S(1)}, u32[]{:S(2)}, u32[]{:S(2)}) collective-permute-start(bf16[256,2048]{1,0:T(8,128)(2,1)S(1)} %copy-done.6), channel_id=1, source_target_pairs={{0,1},{1,0},{2,3},{3,2},{4,5},{5,4},{6,7},{7,6},{8,9},{9,8},{10,11... | collective-permute-start | bytes 3145736 | tf_op jit(solution)/shard_map/ppermute | solution.py:180
  13.8 0.6 %attend.4 = (f32[128,256]{1,0:T(8,128)S(1)}, f32[512,128]{1,0:T(8,128)S(1)}) custom-call(bf16[128,256]{1,0:T(8,128)(2,1)S(1)} %get-tuple-element.15.q_ref, bf16[136,512]{1,0:T(8,128)(2,1)S(1)} %get-tuple-element.16.kv_ref), custom_call_target="tpu_custom_call" | custom-call | flops 1000000000 | bytes 1000000 | tf_op jit(solution)/shard_map/attend/pallas_call | solution.py:135
  14.4 0.6 %collective-permute-done.2.kv_ref = bf16[136,512]{1,0:T(8,128)(2,1)S(1)} collective-permute-done((bf16[136,512]{1,0:T(8,128)(2,1)S(1)}, bf16[136,512]{1,0:T(8,128)(2,1)S(1)}, u32[]{:S(2)}, u32[]{:S(2)}) %collective-permute-start.2) | collective-permute-done | bytes 139296 | tf_op jit(solution)/shard_map/ppermute | solution.py:193
  15.0 0.6 %attend.5 = (f32[128,256]{1,0:T(8,128)S(1)}, f32[512,128]{1,0:T(8,128)S(1)}) custom-call(bf16[128,256]{1,0:T(8,128)(2,1)S(1)} %get-tuple-element.15.q_ref, bf16[136,512]{1,0:T(8,128)(2,1)S(1)} %collective-permute-done.2.kv_ref, f32[128,256]{1,0:T(8,128)S(1)} %get-tuple-element.17.refs_0_, f32[512,128]{1,0:T(8,128)S(1)} %get-tuple-element.18.refs_1_), custom_call_target="tpu_custom_call" | custom-call | flops 1000000000 | bytes 1000000 | tf_op jit(solution)/shard_map/attend/pallas_call | solution.py:135
  15.6 8.9 %collective-permute-done.1.kv_ref = bf16[136,512]{1,0:T(8,128)(2,1)S(1)} collective-permute-done((bf16[136,512]{1,0:T(8,128)(2,1)S(1)}, bf16[136,512]{1,0:T(8,128)(2,1)S(1)}, u32[]{:S(2)}, u32[]{:S(2)}) %collective-permute-start.1) | collective-permute-done | bytes 139296 | tf_op jit(solution)/shard_map/ppermute | solution.py:193
  24.5 0.6 %attend.6 = (f32[128,256]{1,0:T(8,128)S(1)}, f32[512,128]{1,0:T(8,128)S(1)}) custom-call(bf16[128,256]{1,0:T(8,128)(2,1)S(1)} %get-tuple-element.15.q_ref, bf16[136,512]{1,0:T(8,128)(2,1)S(1)} %collective-permute-done.1.kv_ref, f32[128,256]{1,0:T(8,128)S(1)} %get-tuple-element.19.refs_0_, f32[512,128]{1,0:T(8,128)S(1)} %get-tuple-element.20.refs_1_), custom_call_target="tpu_custom_call" | custom-call | flops 1000000000 | bytes 1000000 | tf_op jit(solution)/shard_map/attend/pallas_call | solution.py:135
  25.1 0.0 collective-permute-done.kv_ref
  25.1 1.1 %attend.7 = (bf16[128,256]{1,0:T(8,128)(2,1)S(1)}, f32[512,128]{1,0:T(8,128)}) custom-call(bf16[128,256]{1,0:T(8,128)(2,1)S(1)} %get-tuple-element.15.q_ref, bf16[136,512]{1,0:T(8,128)(2,1)S(1)} %collective-permute-done.kv_ref, f32[128,256]{1,0:T(8,128)S(1)} %get-tuple-element.21.refs_0_, f32[512,128]{1,0:T(8,128)S(1)} %get-tuple-element.22.refs_1_), custom_call_target="tpu_custom_call" | custom-call | flops 1000000000 | bytes 1000000 | tf_op jit(solution)/shard_map/attend/pallas_call | solution.py:135
  26.3 0.0 collective-permute-done.5.refs_5_
  26.3 1.1 %collective-permute-start.7 = (bf16[256,2048]{1,0:T(8,128)(2,1)S(1)}, bf16[256,2048]{1,0:T(8,128)(2,1)S(1)}, u32[]{:S(2)}, u32[]{:S(2)}) collective-permute-start(bf16[256,2048]{1,0:T(8,128)(2,1)S(1)} %collective-permute-done.5.refs_5_), channel_id=1, source_target_pairs={{0,1},{1,0},{2,3},{3,2},{4,5},{5,4},{6,7},{7,6},{8,9},{9,8},{10,11... | collective-permute-start | bytes 3145736 | tf_op jit(solution)/shard_map/ppermute | solution.py:180
  27.4 0.7 %collective-permute-start.3 = (bf16[128,256]{1,0:T(8,128)(2,1)S(1)}, bf16[128,256]{1,0:T(8,128)(2,1)S(1)}, u32[]{:S(2)}, u32[]{:S(2)}) collective-permute-start(bf16[128,256]{1,0:T(8,128)(2,1)S(1)} %get-tuple-element.23.refs_0_), channel_id=1, source_target_pairs={{0,2},{1,3},{2,0},{3,1},{4,6},{5,7},{6,4},{7,5},{8,10},{9,11},{10,... | collective-permute-start | bytes 196616 | tf_op jit(solution)/shard_map/ppermute | solution.py:180
  28.1 3.0 %collective-permute-done.3.refs_1_ = bf16[128,256]{1,0:T(8,128)(2,1)S(1)} collective-permute-done((bf16[128,256]{1,0:T(8,128)(2,1)S(1)}, bf16[128,256]{1,0:T(8,128)(2,1)S(1)}, u32[]{:S(2)}, u32[]{:S(2)}) %collective-permute-start.3) | collective-permute-done | bytes 65568 | tf_op jit(solution)/shard_map/ppermute | solution.py:180
  31.1 0.9 %collective-permute-start.4 = (bf16[128,512]{1,0:T(8,128)(2,1)S(1)}, bf16[128,512]{1,0:T(8,128)(2,1)S(1)}, u32[]{:S(2)}, u32[]{:S(2)}) collective-permute-start(bf16[128,512]{1,0:T(8,128)(2,1)S(1)} %pad_maximum_fusion), channel_id=1, source_target_pairs={{0,1},{1,0},{2,3},{3,2},{4,5},{5,4},{6,7},{7,6},{8,9},{9,8},{10,11... | collective-permute-start | bytes 393224 | tf_op jit(solution)/shard_map/ppermute | solution.py:180
  32.0 1.0 %collective-permute-done.4 = bf16[128,512]{1,0:T(8,128)(2,1)S(1)} collective-permute-done((bf16[128,512]{1,0:T(8,128)(2,1)S(1)}, bf16[128,512]{1,0:T(8,128)(2,1)S(1)}, u32[]{:S(2)}, u32[]{:S(2)}) %collective-permute-start.4) | collective-permute-done | bytes 131104 | tf_op jit(solution)/shard_map/ppermute | solution.py:180
  33.0 0.0 collective-permute-done.6.refs_6_
  33.0 0.0 collective-permute-done.7.refs_7_
  33.0 2.5 %output.1 = bf16[128,2048]{1,0:T(8,128)(2,1)} custom-call(bf16[128,256]{1,0:T(8,128)(2,1)S(1)} %get-tuple-element.23.refs_0_, bf16[128,256]{1,0:T(8,128)(2,1)S(1)} %collective-permute-done.3.refs_1_, bf16[128,256]{1,0:T(8,128)(2,1)S(1)} %get-tuple-element.26.refs_2_, bf16[128,256]{1,0:T(8,128)(2,1)S(1)} %get-tuple-element.25.refs_3_, ...), custom_call_target="tpu_custom_call" | custom-call | flops 2000000000 | bytes 4000000 | tf_op jit(solution)/shard_map/output/pallas_call | solution.py:162
  (2 shorter events, 0.0 us)
Async XLA Ops:
  0.0 1.2 %copy-start.5 = (bf16[4,128]{1,0:T(4,128)(2,1)S(1)}, bf16[4,128]{1,0:T(4,128)(2,1)}, u32[]{:S(2)}) copy-start(bf16[4,128]{1,0:T(4,128)(2,1)} %rate_ref.1) | copy-start | bytes 3076
  0.0 26.3 %collective-permute-start.5 = (bf16[256,2048]{1,0:T(8,128)(2,1)}, bf16[256,2048]{1,0:T(8,128)(2,1)S(1)}, u32[]{:S(2)}, u32[]{:S(2)}) collective-permute-start(bf16[256,2048]{1,0:T(8,128)(2,1)} %refs_4_.1), channel_id=1, source_target_pairs={{0,2},{1,3},{2,0},{3,1},{4,6},{5,7},{6,4},{7,5},{8,10},{9,11},{10,... | collective-permute-start | bytes 3145736 | tf_op jit(solution)/shard_map/ppermute | solution.py:180
  1.2 1.2 %copy-start = (bf16[2048,256]{1,0:T(8,128)(2,1)S(1)}, bf16[2048,256]{1,0:T(8,128)(2,1)}, u32[]{:S(2)}) copy-start(bf16[2048,256]{1,0:T(8,128)(2,1)} %wk_hbm.1) | copy-start | bytes 3145732
  2.4 1.2 %copy-start.1 = (bf16[2048,256]{1,0:T(8,128)(2,1)S(1)}, bf16[2048,256]{1,0:T(8,128)(2,1)}, u32[]{:S(2)}) copy-start(bf16[2048,256]{1,0:T(8,128)(2,1)} %wv_hbm.1) | copy-start | bytes 3145732
  3.7 1.2 %copy-start.2 = (bf16[2048,256]{1,0:T(8,128)(2,1)S(1)}, bf16[2048,256]{1,0:T(8,128)(2,1)}, u32[]{:S(2)}) copy-start(bf16[2048,256]{1,0:T(8,128)(2,1)} %wq_hbm.1) | copy-start | bytes 3145732
  4.9 1.0 %copy-start.3 = (bf16[128,2048]{1,0:T(8,128)(2,1)S(1)}, bf16[128,2048]{1,0:T(8,128)(2,1)}, u32[]{:S(2)}) copy-start(bf16[128,2048]{1,0:T(8,128)(2,1)} %tok_hbm.1) | copy-start | bytes 1572868
  5.9 0.7 %copy-start.4 = (f32[2048]{0:T(1024)S(1)}, f32[2048]{0:T(1024)}, u32[]{:S(2)}) copy-start(f32[2048]{0:T(1024)} %param.8) | copy-start | bytes 24580
  6.6 6.1 %copy-start.6 = (bf16[256,2048]{1,0:T(8,128)(2,1)S(1)}, bf16[256,2048]{1,0:T(8,128)(2,1)}, u32[]{:S(2)}) copy-start(bf16[256,2048]{1,0:T(8,128)(2,1)} %refs_4_.1) | copy-start | bytes 3145732
  8.9 6.2 %collective-permute-start.2 = (bf16[136,512]{1,0:T(8,128)(2,1)S(1)}, bf16[136,512]{1,0:T(8,128)(2,1)S(1)}, u32[]{:S(2)}, u32[]{:S(2)}) collective-permute-start(bf16[136,512]{1,0:T(8,128)(2,1)S(1)} %get-tuple-element.16.kv_ref), channel_id=1, source_target_pairs={{0,4},{4,8},{8,12},{1,5},{5,9},{9,13},{2,6},{6,10},{10,14},{3,7},{... | collective-permute-start | bytes 417800 | tf_op jit(solution)/shard_map/ppermute | solution.py:193
  10.2 14.4 %collective-permute-start.1 = (bf16[136,512]{1,0:T(8,128)(2,1)S(1)}, bf16[136,512]{1,0:T(8,128)(2,1)S(1)}, u32[]{:S(2)}, u32[]{:S(2)}) collective-permute-start(bf16[136,512]{1,0:T(8,128)(2,1)S(1)} %get-tuple-element.16.kv_ref), channel_id=1, source_target_pairs={{0,8},{4,12},{1,9},{5,13},{2,10},{6,14},{3,11},{7,15},{16,24},{20,... | collective-permute-start | bytes 417800 | tf_op jit(solution)/shard_map/ppermute | solution.py:193
  11.5 13.7 %collective-permute-start = (bf16[136,512]{1,0:T(8,128)(2,1)S(1)}, bf16[136,512]{1,0:T(8,128)(2,1)S(1)}, u32[]{:S(2)}, u32[]{:S(2)}) collective-permute-start(bf16[136,512]{1,0:T(8,128)(2,1)S(1)} %get-tuple-element.16.kv_ref), channel_id=1, source_target_pairs={{0,12},{1,13},{2,14},{3,15},{16,28},{17,29},{18,30},{19,31}} | collective-permute-start | bytes 417800 | tf_op jit(solution)/shard_map/ppermute | solution.py:193
  12.8 20.2 %collective-permute-start.6 = (bf16[256,2048]{1,0:T(8,128)(2,1)S(1)}, bf16[256,2048]{1,0:T(8,128)(2,1)S(1)}, u32[]{:S(2)}, u32[]{:S(2)}) collective-permute-start(bf16[256,2048]{1,0:T(8,128)(2,1)S(1)} %copy-done.6), channel_id=1, source_target_pairs={{0,1},{1,0},{2,3},{3,2},{4,5},{5,4},{6,7},{7,6},{8,9},{9,8},{10,11... | collective-permute-start | bytes 3145736 | tf_op jit(solution)/shard_map/ppermute | solution.py:180
  26.3 6.7 %collective-permute-start.7 = (bf16[256,2048]{1,0:T(8,128)(2,1)S(1)}, bf16[256,2048]{1,0:T(8,128)(2,1)S(1)}, u32[]{:S(2)}, u32[]{:S(2)}) collective-permute-start(bf16[256,2048]{1,0:T(8,128)(2,1)S(1)} %collective-permute-done.5.refs_5_), channel_id=1, source_target_pairs={{0,1},{1,0},{2,3},{3,2},{4,5},{5,4},{6,7},{7,6},{8,9},{9,8},{10,11... | collective-permute-start | bytes 3145736 | tf_op jit(solution)/shard_map/ppermute | solution.py:180
  27.4 3.6 %collective-permute-start.3 = (bf16[128,256]{1,0:T(8,128)(2,1)S(1)}, bf16[128,256]{1,0:T(8,128)(2,1)S(1)}, u32[]{:S(2)}, u32[]{:S(2)}) collective-permute-start(bf16[128,256]{1,0:T(8,128)(2,1)S(1)} %get-tuple-element.23.refs_0_), channel_id=1, source_target_pairs={{0,2},{1,3},{2,0},{3,1},{4,6},{5,7},{6,4},{7,5},{8,10},{9,11},{10,... | collective-permute-start | bytes 196616 | tf_op jit(solution)/shard_map/ppermute | solution.py:180
  31.1 1.9 %collective-permute-start.4 = (bf16[128,512]{1,0:T(8,128)(2,1)S(1)}, bf16[128,512]{1,0:T(8,128)(2,1)S(1)}, u32[]{:S(2)}, u32[]{:S(2)}) collective-permute-start(bf16[128,512]{1,0:T(8,128)(2,1)S(1)} %pad_maximum_fusion), channel_id=1, source_target_pairs={{0,1},{1,0},{2,3},{3,2},{4,5},{5,4},{6,7},{7,6},{8,9},{9,8},{10,11... | collective-permute-start | bytes 393224 | tf_op jit(solution)/shard_map/ppermute | solution.py:180
